TPU v7x, 32 devices: a whole 2x2x4 slice. The times are simulated.
32 devices in a mesh: tp: 16 (over z, y, x), dp: 2 (over core).
Axes of the slice: x: 2, y: 2, z: 4, core: 2. Of those that a mesh axis runs over, the one named last changes fastest.
Arguments:
- tokens: bfloat16 [256, 4096], P(None, 'dp'), may hold values from -20 to 20
- norm_gain: float32 [2, 4096], P(None, 'dp'), may hold values from 0.1 to 1.9
- receptance: bfloat16 [2, 4096, 1024], P(None, 'dp', 'tp'), may hold values from -0.09375 to 0.09375
- key_proj: bfloat16 [2, 4096, 1024], P(None, 'dp', 'tp'), may hold values from -0.09375 to 0.09375
- value_proj: bfloat16 [2, 4096, 1024], P(None, 'dp', 'tp'), may hold values from -0.09375 to 0.09375
- decay_proj: bfloat16 [2, 4096, 1024], P(None, 'dp', 'tp'), may hold values from -0.09375 to 0.09375
- rate_proj: bfloat16 [2, 4096, 1024], P(None, 'dp', 'tp'), may hold values from -0.09375 to 0.09375
- gate_proj: bfloat16 [2, 4096, 1024], P(None, 'dp', 'tp'), may hold values from -0.09375 to 0.09375
- decay_base: float32 [2, 1024], P(None, 'tp'), may hold values from -6 to 1
- group_gain: float32 [2, 1024], P(None, 'tp'), may hold values from 0.1 to 1.9
- output_proj: bfloat16 [2, 1024, 4096], P(None, 'tp', 'dp'), may hold values from -0.1875 to 0.1875
- state: float32 [2, 256, 16, 4096], P(None, 'dp', 'tp'), may hold values from -3 to 3
Outputs:
- next_tokens: bfloat16 [256, 4096], P(None, 'dp')
- new_state: float32 [2, 256, 16, 4096], P(None, 'dp', 'tp')
All inputs are finite; a program needn't handle non-finite values.
Results may differ from a plain program's by a relative error of at most 0.0066.
Values may be sent and summed in bfloat16 or wider, within the bound.
A program may use at most 64 MiB of HBM per device.

v0:
```python
import jax
import jax.numpy as jnp
from jax import lax
from jax.sharding import PartitionSpec as P

D = 4096
HEAD = 64
LAYERS = 2


norm_floor = 0.1
group_floor = 0.5


def recurrence(state_block, recept_heads, key_heads, value_heads, decay_heads, rate_heads):
    log_rate = -jax.nn.softplus(-decay_heads) - 0.5
    forget = jnp.exp(-jnp.exp(log_rate))
    learn_rate = jax.nn.sigmoid(rate_heads)
    unit_key = key_heads * lax.rsqrt(jnp.sum(key_heads * key_heads, axis=-1, keepdims=True) + 1.0)
    scaled = key_heads * learn_rate
    removed = jnp.einsum("bhvk,bhk->bhv", state_block, -unit_key, precision=lax.Precision.HIGHEST)
    updated = (
        state_block * forget[:, :, None, :]
        + removed[..., None] * (unit_key * learn_rate)[:, :, None, :]
        + value_heads[..., None] * scaled[:, :, None, :]
    )
    read_out = jnp.einsum("bhvk,bhk->bhv", updated, recept_heads, precision=lax.Precision.HIGHEST)
    centre = read_out - jnp.mean(read_out, axis=-1, keepdims=True)
    normal = centre * lax.rsqrt(jnp.mean(centre * centre, axis=-1, keepdims=True) + group_floor)
    return (updated, normal)


def shards(
    tokens,
    norm_gain,
    receptance,
    key_proj,
    value_proj,
    decay_proj,
    rate_proj,
    gate_proj,
    decay_base,
    group_gain,
    output_proj,
    state,
):
    local_rows = state.shape[1]
    first_row = lax.axis_index("dp") * local_rows
    local_heads = state.shape[2]
    current = tokens
    finals = []
    for section_index in range(LAYERS):
        floats = current.astype(jnp.float32)
        squares = jnp.sum(floats * floats, axis=1)
        normed = (floats * norm_gain[section_index]).astype(jnp.bfloat16)
        part_recept = jnp.dot(normed, receptance[section_index], preferred_element_type=jnp.float32)
        part_key = jnp.dot(normed, key_proj[section_index], preferred_element_type=jnp.float32)
        part_value = jnp.dot(normed, value_proj[section_index], preferred_element_type=jnp.float32)
        part_decay = jnp.dot(normed, decay_proj[section_index], preferred_element_type=jnp.float32)
        part_rate = jnp.dot(normed, rate_proj[section_index], preferred_element_type=jnp.float32)
        part_gate = jnp.dot(normed, gate_proj[section_index], preferred_element_type=jnp.float32)
        totals = lax.psum(squares, "dp")
        own_squares = lax.dynamic_slice_in_dim(totals, first_row, local_rows, 0)
        summed = (
            lax.psum_scatter(part_recept, "dp", scatter_dimension=0, tiled=True),
            lax.psum_scatter(part_key, "dp", scatter_dimension=0, tiled=True),
            lax.psum_scatter(part_value, "dp", scatter_dimension=0, tiled=True),
            lax.psum_scatter(part_decay, "dp", scatter_dimension=0, tiled=True),
            lax.psum_scatter(part_rate, "dp", scatter_dimension=0, tiled=True),
            lax.psum_scatter(part_gate, "dp", scatter_dimension=0, tiled=True),
        )
        inv_rms = lax.rsqrt(own_squares / D + norm_floor)

        def by_head(term):
            rounded = lax.optimization_barrier((inv_rms[:, None] * term).astype(jnp.bfloat16))
            return rounded.astype(jnp.float32).reshape(local_rows, local_heads, HEAD)

        decay_heads = by_head(summed[3]) + decay_base[section_index].reshape(1, local_heads, HEAD)
        updated, normal = recurrence(
            state[section_index].reshape(local_rows, local_heads, HEAD, HEAD),
            by_head(summed[0]),
            by_head(summed[1]),
            by_head(summed[2]),
            decay_heads,
            by_head(summed[4]),
        )
        finals.append(updated.reshape(local_rows, local_heads, HEAD * HEAD))
        gate_value = jax.nn.sigmoid(by_head(summed[5]).reshape(local_rows, local_heads * HEAD))
        mixed_heads = (
            normal.reshape(local_rows, local_heads * HEAD) * group_gain[section_index] * gate_value
        ).astype(jnp.bfloat16)
        weights_out = output_proj[section_index]

        def apply_out(piece, begin, weights_out=weights_out):
            return jnp.dot(piece, weights_out, preferred_element_type=jnp.float32)

        partial_out = apply_out(lax.all_gather(mixed_heads, "dp", axis=0, tiled=True), jnp.int32(0))
        total = lax.psum(partial_out, "tp")
        current = (floats + total).astype(jnp.bfloat16)
    return (current, jnp.stack(finals))


def solution(mesh):
    return jax.shard_map(
        shards,
        mesh=mesh,
        in_specs=(
            P(None, "dp"),
            P(None, "dp"),
            P(None, "dp", "tp"),
            P(None, "dp", "tp"),
            P(None, "dp", "tp"),
            P(None, "dp", "tp"),
            P(None, "dp", "tp"),
            P(None, "dp", "tp"),
            P(None, "tp"),
            P(None, "tp"),
            P(None, "tp", "dp"),
            P(None, "dp", "tp", None),
        ),
        out_specs=(P(None, "dp"), P(None, "dp", "tp", None)),
        check_vma=False,
    )
```

profile of v0, /device:TPU:0, one launch (start us, length us, event | category | flops | bytes accessed | tf_op | source)
XLA Modules:
  0.0 421.7 jit_solution(14630838087907600654)
XLA Ops:
  8.1 2.3 fusion.22
  10.5 2.4 fusion.26
  17.6 8.1 %fusion.77 = (f32[1,128,1,4096]{3,2,1,0:T(1,128)}, f32[1,128,1,4096]{3,2,1,0:T(1,128)}) fusion(f32[2,128,1,4096]{3,2,1,0:T(1,128)} %param.23), kind=kLoop, calls=%fused_computation.119 | loop fusion | bytes 8388608 | tf_op jit(solution)/shard_map/slice | solution.py:80
  26.0 5.0 %copy.45 = f32[1,128,1,4096]{1,3,2,0:T(8,128)S(1)} copy(f32[1,128,1,4096]{3,2,1,0:T(1,128)} %get-tuple-element.7) | data formatting | bytes 4194304
  31.1 2.6 psum.28
  33.8 9.1 %reduce-scatter.17.cloned.1.call-done = f32[128,64]{0,1:T(8,128)} async-done(((f32[256,64]{0,1:T(8,128)}), f32[128,64]{0,1:T(8,128)}) %reduce-scatter.17.cloned.1.call-update) | async-done | bytes 32784 | tf_op jit(solution)/shard_map/reduce_scatter | solution.py:69
  42.8 10.7 %reduce-scatter.21.cloned.1.call-done = f32[128,64]{0,1:T(8,128)} async-done(((f32[256,64]{0,1:T(8,128)}), f32[128,64]{0,1:T(8,128)}) %reduce-scatter.21.cloned.1.call-update) | async-done | bytes 32784 | tf_op jit(solution)/shard_map/reduce_scatter | solution.py:65
  53.6 10.7 %reduce-scatter.23.cloned.1.call-done = f32[128,64]{0,1:T(8,128)} async-done(((f32[256,64]{0,1:T(8,128)}), f32[128,64]{0,1:T(8,128)}) %reduce-scatter.23.cloned.1.call-update) | async-done | bytes 32784 | tf_op jit(solution)/shard_map/reduce_scatter | solution.py:70
  64.3 10.7 %reduce-scatter.13.cloned.1.call-done = f32[128,64]{0,1:T(8,128)} async-done(((f32[256,64]{0,1:T(8,128)}), f32[128,64]{0,1:T(8,128)}) %reduce-scatter.13.cloned.1.call-update) | async-done | bytes 32784 | tf_op jit(solution)/shard_map/reduce_scatter | solution.py:68
  79.2 2.7 fusion.38
  82.0 5.6 %copy.46 = f32[1,128,1,4096]{1,3,2,0:T(8,128)} copy(f32[1,128,1,4096]{3,2,1,0:T(1,128)} %get-tuple-element.6) | data formatting | bytes 4194304
  87.7 122.2 %all-reduce.3.cloned.1.call-done = f32[256,2048]{1,0:T(8,128)} async-done(((f32[256,2048]{1,0:T(8,128)}), f32[256,2048]{1,0:T(8,128)}) %all-reduce.3.cloned.1.call-update) | async-done | bytes 2097168 | tf_op jit(solution)/shard_map/psum | solution.py:98
  214.0 2.4 fusion.14
  216.5 2.3 fusion.12
  225.2 2.6 broadcast_multiply_fusion.2
  227.8 2.6 psum.30
  231.9 10.7 %reduce-scatter.29.cloned.1.call-done = f32[128,64]{0,1:T(8,128)} async-done(((f32[256,64]{0,1:T(8,128)}), f32[128,64]{0,1:T(8,128)}) %reduce-scatter.29.cloned.1.call-update) | async-done | bytes 32784 | tf_op jit(solution)/shard_map/reduce_scatter | solution.py:69
  242.6 11.5 %reduce-scatter.33.cloned.1.call-done = f32[128,64]{0,1:T(8,128)} async-done(((f32[256,64]{0,1:T(8,128)}), f32[128,64]{0,1:T(8,128)}) %reduce-scatter.33.cloned.1.call-update) | async-done | bytes 32784 | tf_op jit(solution)/shard_map/reduce_scatter | solution.py:65
  254.1 10.7 %reduce-scatter.35.cloned.1.call-done = f32[128,64]{0,1:T(8,128)} async-done(((f32[256,64]{0,1:T(8,128)}), f32[128,64]{0,1:T(8,128)}) %reduce-scatter.35.cloned.1.call-update) | async-done | bytes 32784 | tf_op jit(solution)/shard_map/reduce_scatter | solution.py:70
  264.8 10.9 %reduce-scatter.25.cloned.1.call-done = f32[128,64]{0,1:T(8,128)} async-done(((f32[256,64]{0,1:T(8,128)}), f32[128,64]{0,1:T(8,128)}) %reduce-scatter.25.cloned.1.call-update) | async-done | bytes 32784 | tf_op jit(solution)/shard_map/reduce_scatter | solution.py:68
  281.7 2.7 fusion.30
  292.9 10.1 %copy.24 = f32[2,128,1,4096]{3,2,1,0:T(1,128)} copy(f32[2,128,1,4096]{1,3,2,0:T(8,128)} %pad_maximum_fusion) | data formatting | bytes 8388608
  303.1 109.3 %all-reduce.5.cloned.1.call-done = f32[256,2048]{1,0:T(8,128)} async-done(((f32[256,2048]{1,0:T(8,128)}), f32[256,2048]{1,0:T(8,128)}) %all-reduce.5.cloned.1.call-update) | async-done | bytes 2097168 | tf_op jit(solution)/shard_map/psum | solution.py:98
  412.4 2.8 fusion.5
  (109 shorter events, 36.4 us)
Async XLA Ops:
  7.2 5.8 %copy-start.3 = (bf16[256,2048]{1,0:T(8,128)(2,1)S(1)}, bf16[256,2048]{1,0:T(8,128)(2,1)}, u32[]{:S(2)}) copy-start(bf16[256,2048]{1,0:T(8,128)(2,1)} %param.12) | copy-start | bytes 3145732
  7.2 5.8 %copy-start.9 = (bf16[2,2048,64]{1,2,0:T(8,128)(2,1)S(1)}, bf16[2,2048,64]{1,2,0:T(8,128)(2,1)}, u32[]{:S(2)}) copy-start(bf16[2,2048,64]{1,2,0:T(8,128)(2,1)} %param.18) | copy-start | bytes 1572868
  7.2 26.6 %reduce-scatter.19.cloned.1.call-start = ((), (), s32[]{:S(2)}) async-start(), calls=%async_computation.15 | async-start | bytes 98304 | tf_op jit(solution)/shard_map/reduce_scatter | solution.py:67
  10.4 3.7 copy-start.10
  10.5 23.3 %reduce-scatter.15.cloned.1.call-start = ((), (), s32[]{:S(2)}) async-start(), calls=%async_computation.13 | async-start | bytes 98304 | tf_op jit(solution)/shard_map/reduce_scatter | solution.py:66
  12.9 2.4 copy-start.11
  12.9 29.9 %reduce-scatter.17.cloned.1.call-start = ((), (), s32[]{:S(2)}) async-start(), calls=%async_computation.14 | async-start | bytes 98304 | tf_op jit(solution)/shard_map/reduce_scatter | solution.py:69
  14.1 2.4 copy-start.12
  14.1 39.5 %reduce-scatter.21.cloned.1.call-start = ((), (), s32[]{:S(2)}) async-start(), calls=%async_computation.16 | async-start | bytes 98304 | tf_op jit(solution)/shard_map/reduce_scatter | solution.py:65
  15.2 49.1 %reduce-scatter.23.cloned.1.call-start = ((), (), s32[]{:S(2)}) async-start(), calls=%async_computation.17 | async-start | bytes 98304 | tf_op jit(solution)/shard_map/reduce_scatter | solution.py:70
  16.4 58.7 %reduce-scatter.13.cloned.1.call-start = ((), (), s32[]{:S(2)}) async-start(), calls=%async_computation.12 | async-start | bytes 98304 | tf_op jit(solution)/shard_map/reduce_scatter | solution.py:68
  17.5 8.2 %copy-start.6 = (f32[2,64]{1,0:T(2,128)S(1)}, f32[2,64]{1,0:T(2,128)}, u32[]{:S(2)}) copy-start(f32[2,64]{1,0:T(2,128)} %param.20) | copy-start | bytes 1540
  17.6 8.1 %copy-start.7 = (f32[2,64]{1,0:T(2,128)S(1)}, f32[2,64]{1,0:T(2,128)}, u32[]{:S(2)}) copy-start(f32[2,64]{1,0:T(2,128)} %param.21) | copy-start | bytes 1540
  17.6 192.3 %all-reduce.3.cloned.1.call-start = ((), (), s32[]{:S(2)}) async-start(), calls=%async_computation.18 | async-start | bytes 4194304 | tf_op jit(solution)/shard_map/psum | solution.py:98
  82.0 148.6 %reduce-scatter.31.cloned.1.call-start = ((), (), s32[]{:S(2)}) async-start(), calls=%async_computation.22 | async-start | bytes 98304 | tf_op jit(solution)/shard_map/reduce_scatter | solution.py:67
  209.9 3.0 copy-start.8
  214.0 5.0 %copy-start.5 = (bf16[256,2048]{1,0:T(8,128)(2,1)S(1)}, bf16[256,2048]{1,0:T(8,128)(2,1)}, u32[]{:S(2)}) copy-start(bf16[256,2048]{1,0:T(8,128)(2,1)} %copy-done.4) | copy-start | bytes 3145732
  214.0 17.9 %reduce-scatter.27.cloned.1.call-start = ((), (), s32[]{:S(2)}) async-start(), calls=%async_computation.20 | async-start | bytes 98304 | tf_op jit(solution)/shard_map/reduce_scatter | solution.py:66
  216.5 26.1 %reduce-scatter.29.cloned.1.call-start = ((), (), s32[]{:S(2)}) async-start(), calls=%async_computation.21 | async-start | bytes 98304 | tf_op jit(solution)/shard_map/reduce_scatter | solution.py:69
  218.9 35.2 %reduce-scatter.33.cloned.1.call-start = ((), (), s32[]{:S(2)}) async-start(), calls=%async_computation.23 | async-start | bytes 98304 | tf_op jit(solution)/shard_map/reduce_scatter | solution.py:65
  221.0 43.8 %reduce-scatter.35.cloned.1.call-start = ((), (), s32[]{:S(2)}) async-start(), calls=%async_computation.24 | async-start | bytes 98304 | tf_op jit(solution)/shard_map/reduce_scatter | solution.py:70
  223.1 52.6 %reduce-scatter.25.cloned.1.call-start = ((), (), s32[]{:S(2)}) async-start(), calls=%async_computation.19 | async-start | bytes 98304 | tf_op jit(solution)/shard_map/reduce_scatter | solution.py:68
  225.2 187.2 %all-reduce.5.cloned.1.call-start = ((), (), s32[]{:S(2)}) async-start(), calls=%async_computation.25 | async-start | bytes 4194304 | tf_op jit(solution)/shard_map/psum | solution.py:98
  275.7 3.2 copy-start
  (3 other events, 4.2 us)
Sparse Core Ops, SparseCore 0:
  10.8 10.2 reduce-scatter.18
  23.2 8.6 reduce-scatter.14
  34.2 8.6 reduce-scatter.16
  44.9 8.6 reduce-scatter.20
  55.6 8.6 reduce-scatter.22
  66.4 8.6 reduce-scatter.12
  82.1 127.7 all-reduce.2
  214.1 6.7 reduce-scatter.30
  223.1 8.7 reduce-scatter.26
  233.9 8.6 reduce-scatter.28
  245.4 8.6 reduce-scatter.32
  256.1 8.6 reduce-scatter.34
  267.0 8.6 reduce-scatter.24
  284.6 127.7 all-reduce.4
where the time goes:
time: 423 us; the launch traced here: 422 us
  waiting for transfers between devices  318 us (75%)
  local copies, waits for them, and re-layouts  33.9 us (8%)
  matrix products  26.4 us (6%)
  other arithmetic  19.5 us (5%)
  between operations  14.2 us (3%)
  blocking collectives  8.96 us (2%)
    psum x2, waiting for transfers between devices, shards(): total = lax.psum(partial_out, 'tp')  231 us
    unnamed x29, local copies, waits for them, and re-layouts  24.5 us
    reduce_scatter x2, waiting for transfers between devices, shards(): lax.psum_scatter(part_recept, 'dp', scatter_dimension=0, tiled=True)  22.2 us
    reduce_scatter x2, waiting for transfers between devices, shards(): lax.psum_scatter(part_decay, 'dp', scatter_dimension=0, tiled=True)  21.6 us
    reduce_scatter x2, waiting for transfers between devices, shards(): lax.psum_scatter(part_gate, 'dp', scatter_dimension=0, tiled=True)  21.5 us
    reduce_scatter x2, waiting for transfers between devices, shards(): lax.psum_scatter(part_rate, 'dp', scatter_dimension=0, tiled=True)  19.8 us
  transfers between devices with their start and end apart: 14, of which 11 were waited for; matrix products, arithmetic and copies ran while one was open for 13% of the time, Pallas kernels for 0%

commit v1 on v0

--- a/solution.py
+++ b/solution.py
@@ -1,6 +1,10 @@
+import functools
+
 import jax
 import jax.numpy as jnp
 from jax import lax
+from jax.experimental import pallas as pl
+from jax.experimental.pallas import tpu as pltpu
 from jax.sharding import PartitionSpec as P
 
 D = 4096
@@ -100,9 +104,397 @@
     return (current, jnp.stack(finals))
 
 
+MESH = pl.DeviceIdType.MESH
+NT = (((1,), (1,)), ((), ()))
+VMEM_LIMIT = 60 * 1024 * 1024
+
+
+def remote(src, dst, send, recv, t, d):
+    return pltpu.make_async_remote_copy(
+        src_ref=src, dst_ref=dst, send_sem=send, recv_sem=recv, device_id={"tp": t, "dp": d}, device_id_type=MESH
+    )
+
+
+def greet(peers):
+    barrier = pltpu.get_barrier_semaphore()
+    for t, d in peers:
+        pl.semaphore_signal(barrier, inc=1, device_id={"tp": t, "dp": d}, device_id_type=MESH)
+    pl.semaphore_wait(barrier, len(peers))
+
+
+class Lanes:
+    def __init__(self, tp):
+        self.t, self.d = lax.axis_index("tp"), lax.axis_index("dp")
+        self.nz = tp // 4
+        self.x, self.y, self.z = lax.rem(self.t, 2), lax.rem(self.t // 2, 2), self.t // 4
+
+    def at(self, x, y, dz):
+        return lax.rem(self.z + dz, self.nz) * 4 + y * 2 + x
+
+    def peers(self):
+        near = [self.at(1 - self.x, self.y, 0), self.at(self.x, 1 - self.y, 0)]
+        return [(p, self.d) for p in near + [self.at(self.x, self.y, dz) for dz in range(1, self.nz)]]
+
+
+def gather(lanes, buf, send, recv):
+    x, y, nz, d = lanes.x, lanes.y, lanes.nz, lanes.d
+    xp, yp = lanes.at(1 - x, y, 0), lanes.at(x, 1 - y, 0)
+    started = []
+    count = [0, 0]
+
+    def put(half, block, target):
+        op = remote(buf.at[half, block], buf.at[half, block], send.at[half, count[half]], recv.at[half, block], target, d)
+        count[half] += 1
+        op.start()
+        started.append(op)
+
+    def got(half, block):
+        remote(buf.at[half, block], buf.at[half, block], send.at[half, 0], recv.at[half, block], xp, d).wait_recv()
+
+    zs = list(range(1, nz))
+    own = lanes.t
+    put(0, own, yp)
+    for dz in zs:
+        put(1, own, lanes.at(x, y, dz))
+        put(0, own, lanes.at(x, y, dz))
+    put(1, own, xp)
+    put(1, own, yp)
+    put(0, own, xp)
+    got(0, yp)
+    for dz in zs:
+        put(0, yp, lanes.at(x, y, dz))
+    put(0, yp, xp)
+    got(1, xp)
+    put(1, xp, yp)
+    for dz in zs:
+        block = lanes.at(x, y, dz)
+        got(1, block)
+        put(1, block, xp)
+        put(1, block, yp)
+        got(0, block)
+        put(0, block, xp)
+    for dz in zs:
+        block = lanes.at(x, 1 - y, dz)
+        got(0, block)
+        put(0, block, xp)
+        block = lanes.at(1 - x, y, dz)
+        got(1, block)
+        put(1, block, yp)
+    for dz in range(nz):
+        for k in range(2):
+            got(0, lanes.at(1 - x, k, dz))
+            got(1, lanes.at(k, 1 - y, dz))
+    for op in started:
+        op.wait_send()
+
+
+def first_kernel(
+    tp, tok, gain, wr, wk, wv, wd, wa, wg, wo, proj, near, w1, gain1, outw,
+    tokv, w0, part, inbox, load, send, recv, a2a_send, a2a_recv,
+):
+    lanes = Lanes(tp)
+    t, d = lanes.t, lanes.d
+    per = tp // 2
+    rows, feats = tok.shape
+    mine = rows // 2
+    cols = feats // per
+    weights = (wr, wk, wv, wd, wa, wg)
+    loads = [pltpu.make_async_copy(tok, tokv, load.at[0])]
+    for i, w in enumerate(weights):
+        loads.append(pltpu.make_async_copy(w.at[0], w0.at[pl.ds(i * HEAD, HEAD)], load.at[1 + i]))
+        loads.append(pltpu.make_async_copy(w.at[1], w1.at[d, pl.ds(i * HEAD, HEAD)], load.at[7 + i]))
+    for op in loads:
+        op.start()
+    greet([(lax.rem(t + k, tp), d) for k in range(1, tp)] + [(t, 1 - d)])
+
+    def spread(c):
+        target = d * per + c
+        return remote(wo.at[:, :, pl.ds(c * cols, cols)], outw.at[t], a2a_send.at[c], a2a_recv.at[t], target, d)
+
+    for c in range(per):
+        @pl.when(d * per + c != t)
+        def _(c=c):
+            spread(c).start()
+
+        @pl.when(d * per + c == t)
+        def _(c=c):
+            pltpu.make_async_copy(wo.at[:, :, pl.ds(c * cols, cols)], outw.at[t], a2a_send.at[c]).start()
+
+    loads[0].wait()
+    slot = lax.rem(t, per)
+    there = (1 - d) * mine
+    pair = [
+        remote(
+            tokv.at[pl.ds(pl.multiple_of(there, mine), mine), pl.ds(pl.multiple_of(slot * cols, cols), cols)],
+            near, send.at[0], recv.at[0], t, 1 - d,
+        ),
+        remote(gain, gain1.at[d], send.at[1], recv.at[1], t, 1 - d),
+    ]
+    for i, w in enumerate(weights):
+        pair.append(remote(w.at[1], w1.at[d, pl.ds(i * HEAD, HEAD)], send.at[2 + i], recv.at[2 + i], t, 1 - d))
+    pair[0].start()
+    pair[1].start()
+    gain1[pl.ds(d, 1)] = gain[...][None]
+
+    floats = tokv[...].astype(jnp.float32)
+    squares = jnp.sum(floats * floats, axis=1, keepdims=True)
+    normed = (floats * gain[0:1, :]).astype(jnp.bfloat16)
+    for i in range(6):
+        loads[1 + 2 * i].wait()
+    width = 6 * HEAD
+    part[:, 0:width] = lax.dot_general(normed, w0[...], NT, preferred_element_type=jnp.float32)
+    part[:, width:] = jnp.broadcast_to(squares, (rows, part.shape[1] - width))
+    swap = remote(part.at[pl.ds(pl.multiple_of(there, mine), mine)], inbox, send.at[8], recv.at[8], t, 1 - d)
+    swap.start()
+    for op in pair[2:]:
+        op.start()
+    swap.wait_recv()
+    total = part[pl.ds(pl.multiple_of(d * mine, mine), mine), :] + inbox[...]
+    inv = lax.rsqrt(total[:, width : width + 1] / (feats * 2) + norm_floor)
+    proj[...] = (inv * total[:, :width]).astype(jnp.bfloat16)
+
+    pair[0].wait_recv()
+    own = tokv[pl.ds(pl.multiple_of(d * mine, mine), mine), pl.ds(pl.multiple_of(slot * cols, cols), cols)]
+    here = (t // per == d).astype(jnp.float32)
+    near[...] = (own.astype(jnp.float32) * here + near[...].astype(jnp.float32) * (1.0 - here)).astype(jnp.bfloat16)
+
+    forward = remote(outw, outw, send.at[9], recv.at[9], t, 1 - d)
+
+    @pl.when(t // per == d)
+    def _():
+        for k in range(1, tp):
+            source = lax.rem(t + k, tp)
+            remote(outw.at[source], outw.at[source], a2a_send.at[0], a2a_recv.at[source], t, 1 - d).wait_recv()
+        pltpu.make_async_copy(outw.at[t], outw.at[t], a2a_send.at[slot]).wait()
+        forward.start()
+
+    for c in range(per):
+        @pl.when(d * per + c != t)
+        def _(c=c):
+            spread(c).wait_send()
+
+    @pl.when(t // per == d)
+    def _():
+        forward.wait_send()
+
+    @pl.when(t // per != d)
+    def _():
+        forward.wait_recv()
+
+    for op in pair[1:]:
+        op.wait_recv()
+    for op in pair:
+        op.wait_send()
+    swap.wait_send()
+    for i in range(6):
+        loads[2 + 2 * i].wait()
+
+
+def state_kernel(proj, base, ggain, state, *rest):
+    new, mixed = rest[-2], rest[-1]
+    seqs = proj.shape[0]
+    lines = state.shape[1] // seqs
+    wide = 2 * HEAD
+
+    def piece(i):
+        return proj[:, i * HEAD : (i + 1) * HEAD].astype(jnp.float32)
+
+    recept, key, value, decay, rate, gate = [piece(i) for i in range(6)]
+    forget = jnp.exp(-jnp.exp(-jax.nn.softplus(-(decay + base[...])) - 0.5))
+    scale = lax.rsqrt(jnp.sum(key * key, axis=-1, keepdims=True) + 1.0)
+    learned = key * jax.nn.sigmoid(rate)
+
+    def spread(row):
+        both = jnp.concatenate([row, row], axis=-1)
+        return jnp.broadcast_to(both[:, None, :], (seqs, lines, wide))
+
+    def iota(shape, axis):
+        return lax.broadcasted_iota(jnp.int32, shape, axis)
+
+    old = state[0].reshape(seqs, lines, wide)
+    lane, col = iota((wide, wide), 0), iota((wide, wide), 1)
+    same = (lane // HEAD == col // HEAD).astype(jnp.bfloat16)
+    odd = ((lane < HEAD) & (lane % 2 == col // HEAD)).astype(jnp.bfloat16)
+    turn = (lane // HEAD == col % 2).astype(jnp.bfloat16)
+    mask = (iota((lines, wide), 1) % HEAD) // 2 == iota((lines, wide), 0)
+
+    def split(term):
+        flat = term.reshape(seqs * lines, wide)
+        high = flat.astype(jnp.bfloat16)
+        return [high, (flat - high.astype(jnp.float32)).astype(jnp.bfloat16)]
+
+    removed = split(old * spread(key * (-scale * scale)))
+    chosen = jnp.where(mask[None], spread(value), 0.0).reshape(seqs * lines, wide).astype(jnp.bfloat16)
+    rank = jnp.dot(
+        jnp.concatenate(removed + [chosen], axis=1), jnp.concatenate([same, same, odd], axis=0),
+        preferred_element_type=jnp.float32,
+    ).reshape(seqs, lines, wide)
+    updated = old * spread(forget) + rank * spread(learned)
+    new[0] = updated.reshape(seqs * lines, wide)
+    read = jnp.dot(
+        jnp.concatenate(split(updated * spread(recept)), axis=1), jnp.concatenate([turn, turn], axis=0),
+        preferred_element_type=jnp.float32,
+    ).reshape(seqs, lines, wide)
+    read = jnp.sum(jnp.where(mask[None], read, 0.0), axis=1)[:, :HEAD]
+    centre = read - jnp.mean(read, axis=-1, keepdims=True)
+    normal = centre * lax.rsqrt(jnp.mean(centre * centre, axis=-1, keepdims=True) + group_floor)
+    mixed[...] = (normal * ggain[...] * jax.nn.sigmoid(gate)).astype(jnp.bfloat16)
+
+
+def project_out(lanes, tp, layer, mixed, outw, near, mg, we, send, recv):
+    mine, half = mixed.shape[0], mixed.shape[0] // 2
+    cols = near.shape[1]
+    heads = jnp.concatenate([mixed[0:half, :], mixed[half:mine, :]], axis=1)
+    for k in range(2):
+        mg[k, lanes.t] = heads[k * half // 2 : (k + 1) * half // 2]
+    greet(lanes.peers() + [(lanes.t, 1 - lanes.d)])
+    we[...] = jnp.zeros_like(we)
+    for k in range(tp):
+        block = outw[k, layer]
+        we[k * 2 * HEAD : k * 2 * HEAD + HEAD, 0:cols] = block
+        we[k * 2 * HEAD + HEAD : (k + 1) * 2 * HEAD, cols : 2 * cols] = block
+    gather(lanes, mg, send, recv)
+    packed = jnp.concatenate(
+        [jnp.concatenate([mg[k, j] for j in range(tp)], axis=1) for k in range(2)], axis=0
+    )
+    out = jnp.dot(packed, we[...], preferred_element_type=jnp.float32)
+    out = jnp.concatenate([out[:, :cols], out[:, cols:]], axis=0)
+    return (near[...].astype(jnp.float32) + out).astype(jnp.bfloat16)
+
+
+def middle_kernel(tp, mixed, outw, near, w1, gain1, proj, after, mg, we, xg, send, recv, xsend, xrecv):
+    lanes = Lanes(tp)
+    current = project_out(lanes, tp, 0, mixed, outw, near, mg, we, send, recv)
+    after[...] = current
+    lane = current.shape[1] // 2
+    for k in range(2):
+        xg[k, lanes.t] = current[:, k * lane : (k + 1) * lane]
+    gather(lanes, xg, xsend, xrecv)
+    per = tp // 2
+    squares, part = 0.0, 0.0
+    for e in range(2):
+        floats = jnp.concatenate([xg[k, e * per + j] for j in range(per) for k in range(2)], axis=1).astype(jnp.float32)
+        squares = squares + jnp.sum(floats * floats, axis=1, keepdims=True)
+        normed = (floats * gain1[e, 1:2, :]).astype(jnp.bfloat16)
+        part = part + lax.dot_general(normed, w1[e], NT, preferred_element_type=jnp.float32)
+    inv = lax.rsqrt(squares / (w1.shape[0] * w1.shape[2]) + norm_floor)
+    proj[...] = (inv * part).astype(jnp.bfloat16)
+
+
+def last_kernel(tp, mixed, outw, near, final, mg, we, xg, xo, send, recv, xsend, xrecv, osend, orecv):
+    lanes = Lanes(tp)
+    current = project_out(lanes, tp, 1, mixed, outw, near, mg, we, send, recv)
+    mine, lane = current.shape[0], current.shape[1] // 2
+    d, per = lanes.d, tp // 2
+    for k in range(2):
+        xg[k, lanes.t] = current[:, k * lane : (k + 1) * lane]
+    gather(lanes, xg, xsend, xrecv)
+    swap = remote(xg.at[:, pl.ds((1 - d) * per, per)], xo, osend, orecv, lanes.t, 1 - d)
+    swap.start()
+    for j in range(per):
+        for k in range(2):
+            at = (2 * j + k) * lane
+            final[pl.ds(pl.multiple_of(d * mine, mine), mine), at : at + lane] = xg[k, d * per + j]
+    swap.wait()
+    for j in range(per):
+        for k in range(2):
+            at = (2 * j + k) * lane
+            final[pl.ds(pl.multiple_of((1 - d) * mine, mine), mine), at : at + lane] = xo[k, j]
+
+
+def fast(tp, tokens, norm_gain, projections, decay_base, group_gain, output_proj, state):
+    rows, feats = tokens.shape
+    mine, per = rows // 2, tp // 2
+    cols = feats // per
+    width = 6 * HEAD
+    lines = HEAD * HEAD // (2 * HEAD)
+    bf, f32 = jnp.bfloat16, jnp.float32
+    shape = jax.ShapeDtypeStruct
+    dma = pltpu.SemaphoreType.DMA
+    vm, anywhere = pl.BlockSpec(memory_space=pltpu.VMEM), pl.BlockSpec(memory_space=pl.ANY)
+    turned = [jnp.swapaxes(w, 1, 2) for w in projections]
+    flat = state.reshape(LAYERS, mine * lines, 2 * HEAD)
+
+    def params(number):
+        return pltpu.CompilerParams(collective_id=number, has_side_effects=True, vmem_limit_bytes=VMEM_LIMIT)
+
+    proj, near, w1, gain1, outw = pl.pallas_call(
+        functools.partial(first_kernel, tp),
+        out_shape=(
+            shape((mine, width), bf), shape((mine, cols), bf), shape((2, width, feats), bf),
+            shape((2, LAYERS, feats), f32), shape((tp, LAYERS, HEAD, cols), bf),
+        ),
+        in_specs=[anywhere, vm] + [anywhere] * 7,
+        out_specs=(vm,) * 5,
+        scratch_shapes=[
+            pltpu.VMEM((rows, feats), bf), pltpu.VMEM((width, feats), bf), pltpu.VMEM((rows, width + 128), f32),
+            pltpu.VMEM((mine, width + 128), f32), dma((13,)), dma((10,)), dma((10,)), dma((per,)), dma((tp,)),
+        ],
+        compiler_params=params(0),
+        name="first",
+    )(tokens, norm_gain, *turned, output_proj)
+
+    seqs = min(mine, 32)
+
+    def recur(layer, proj, filled):
+        extra = [] if filled is None else [filled]
+        return pl.pallas_call(
+            state_kernel,
+            grid=(mine // seqs,),
+            out_shape=(shape(flat.shape, f32), shape((mine, HEAD), bf)),
+            in_specs=[
+                pl.BlockSpec((seqs, width), lambda i: (i, 0)),
+                pl.BlockSpec((1, HEAD), lambda i: (0, 0)),
+                pl.BlockSpec((1, HEAD), lambda i: (0, 0)),
+                pl.BlockSpec((1, seqs * lines, 2 * HEAD), lambda i: (layer, i, 0)),
+            ] + [anywhere] * len(extra),
+            out_specs=(
+                pl.BlockSpec((1, seqs * lines, 2 * HEAD), lambda i: (layer, i, 0)),
+                pl.BlockSpec((seqs, HEAD), lambda i: (i, 0)),
+            ),
+            input_output_aliases={4: 0} if extra else {},
+            compiler_params=pltpu.CompilerParams(vmem_limit_bytes=VMEM_LIMIT),
+            name=f"state{layer}",
+        )(proj, decay_base[layer : layer + 1], group_gain[layer : layer + 1], flat, *extra)
+
+    filled, mixed = recur(0, proj, None)
+    common = [pltpu.VMEM((2, tp, mine // 4, 2 * HEAD), bf), pltpu.VMEM((tp * 2 * HEAD, 2 * cols), bf),
+              pltpu.VMEM((2, tp, mine, cols // 2), bf)]
+    sems = [dma((2, tp)), dma((2, tp)), dma((2, tp)), dma((2, tp))]
+    proj, near = pl.pallas_call(
+        functools.partial(middle_kernel, tp),
+        out_shape=(shape((mine, width), bf), shape((mine, cols), bf)),
+        in_specs=[vm] * 5,
+        out_specs=(vm,) * 2,
+        scratch_shapes=common + sems,
+        compiler_params=params(1),
+        name="middle",
+    )(mixed, outw, near, w1, gain1)
+    filled, mixed = recur(1, proj, filled)
+    final = pl.pallas_call(
+        functools.partial(last_kernel, tp),
+        out_shape=shape((rows, feats), bf),
+        in_specs=[vm] * 3,
+        out_specs=vm,
+        scratch_shapes=common + [pltpu.VMEM((2, per, mine, cols // 2), bf)] + sems + [dma, dma],
+        compiler_params=params(2),
+        name="last",
+    )(mixed, outw, near)
+    return (final, filled.reshape(state.shape))
+
+
+def step(tp, dp, tokens, norm_gain, *rest):
+    projections, (decay_base, group_gain, output_proj, state) = rest[:6], rest[6:]
+    rows, feats = tokens.shape
+    fits = dp == 2 and tp % 8 == 0 and state.shape[2] == 1 and state.shape[1] % 64 == 0 and (feats * dp // tp) % 256 == 0
+    if fits:
+        return fast(tp, tokens, norm_gain, projections, decay_base, group_gain, output_proj, state)
+    return shards(tokens, norm_gain, *rest)
+
+
 def solution(mesh):
     return jax.shard_map(
-        shards,
+        functools.partial(step, mesh.shape["tp"], mesh.shape["dp"]),
         mesh=mesh,
         in_specs=(
             P(None, "dp"),

time: 423 us -> 102 us (0.24)
  waiting for transfers between devices: 318 us -> 0 us
  Pallas kernels: 0 us -> 97.5 us
  local copies, waits for them, and re-layouts: 33.9 us -> 3.65 us
  matrix products: 26.4 us -> 0 us
  other arithmetic: 19.5 us -> 0 us
  between operations: 14.2 us -> 0.66 us
  blocking collectives: 8.96 us -> 0 us
    psum x2 -> x0, waiting for transfers between devices: 231 us -> none  [shards(): total = lax.psum(partial_out, 'tp')]
    pallas_call x0 -> x5, Pallas kernels: none -> 97.5 us  [the longest x1 34.8 us: fast(): pl.pallas_call(functools.partial(middle_kernel, tp), out_shape=(shape((mi...]
    reduce_scatter x12 -> x0, waiting for transfers between devices: 86.4 us -> none  [the longest x2 22.2 us: shards(): lax.psum_scatter(part_recept, 'dp', scatter_dimension=0, tiled=True)]
    dot_general x14 -> x0, matrix products: 26.4 us -> none  [the longest x2 5.48 us: apply_out(): return jnp.dot(piece, weights_out, preferred_element_type=jnp.float32)]
    unnamed x29 -> x1, local copies, waits for them, and re-layouts: 24.5 us -> 2.3 us
    slice x2 -> x1, local copies, waits for them, and re-layouts: 8.93 us -> 1.35 us  [recur(): group_gain[layer:layer + 1]]
    psum x2 -> x0, blocking collectives: 5.26 us -> none  [shards(): totals = lax.psum(squares, 'dp')]
    convert_element_type x7 -> x0, other arithmetic: 4.88 us -> none  [the longest x1 2.85 us: shards(): current = (floats + total).astype(jnp.bfloat16)]
  transfers between devices with their start and end apart: 14 -> 0, of which waited for: 11 -> 0; matrix products, arithmetic and copies ran while one was open for 13% -> 0% of each run, Pallas kernels for 0% -> 0%
where the time goes in v1:
time: 102 us
  Pallas kernels  97.5 us (96%)
  local copies, waits for them, and re-layouts  3.65 us (4%)
    pallas_call x1, Pallas kernels, fast(): pl.pallas_call(functools.partial(middle_kernel, tp), out_shape=(shape((mi...  34.8 us
    pallas_call x1, Pallas kernels, fast(): pl.pallas_call(functools.partial(last_kernel, tp), out_shape=shape((rows,...  28.4 us
    pallas_call x1, Pallas kernels, fast(): pl.pallas_call(functools.partial(first_kernel, tp), out_shape=(shape((min...  20.6 us
    pallas_call x2, Pallas kernels, recur(): pl.pallas_call(state_kernel, grid=(mine // seqs,), out_shape=(shape(flat....  13.7 us
    unnamed x1, local copies, waits for them, and re-layouts  2.3 us

profile of v1, /device:TPU:0, one launch (start us, length us, event | category | flops | bytes accessed | tf_op | source)
XLA Modules:
  0.0 101.8 jit_solution(5056516768359258418)
XLA Ops:
  0.6 1.4 %fusion = (f32[1,64]{1,0:T(1,128)}, f32[1,64]{1,0:T(1,128)}, f32[1,64]{1,0:T(1,128)}, f32[1,64]{1,0:T(1,128)}) fusion(f32[2,64]{1,0:T(2,128)} %param.21, f32[2,64]{1,0:T(2,128)} %param.20), kind=kLoop, calls=%fused_computation | loop fusion | bytes 2048 | tf_op jit(solution)/shard_map/slice | solution.py:458
  2.0 20.6 %first.1 = (bf16[128,384]{1,0:T(8,128)(2,1)}, bf16[128,256]{1,0:T(8,128)(2,1)}, bf16[2,384,2048]{2,1,0:T(8,128)(2,1)}, f32[2,2,2048]{2,1,0:T(2,128)}, bf16[16,2,64,256]{3,2,1,0:T(8,128)(2,1)}) custom-call(bf16[256,2048]{1,0:T(8,128)(2,1)} %tok.1, f32[2,2048]{1,0:T(2,128)} %gain.1, bf16[2,64,2048]{2,1,0:T(8,128)(2,1)} %bitcast.11, ...), custom_call_target="tpu_custom_call" | custom-call | tf_op jit(solution)/shard_map/first/pallas_call | solution.py:421
  22.6 6.9 %state0.1 = (f32[2,4096,128]{2,1,0:T(8,128)}, bf16[128,64]{1,0:T(8,128)(2,1)}) custom-call(bf16[128,384]{1,0:T(8,128)(2,1)} %get-tuple-element.13.proj, f32[1,64]{1,0:T(1,128)} %get-tuple-element.30.base, f32[1,64]{1,0:T(1,128)} %get-tuple-element.27.ggain, f32[2,4096,128]{2,1,0:T(8,128)} %bitcast.8), custom_call_target="tpu_custom_call" | custom-call | tf_op jit(solution)/shard_map/state0/pallas_call | solution.py:441
  29.5 34.8 %middle.1 = (bf16[128,384]{1,0:T(8,128)(2,1)}, bf16[128,256]{1,0:T(8,128)(2,1)}) custom-call(bf16[128,64]{1,0:T(8,128)(2,1)} %get-tuple-element.14.mixed, bf16[16,2,64,256]{3,2,1,0:T(8,128)(2,1)} %get-tuple-element.15.outw, bf16[128,256]{1,0:T(8,128)(2,1)} %get-tuple-element.16.near, bf16[2,384,2048]{2,1,0:T(8,128)(2,1)} %get-tuple-element.17.w1, ...), custom_call_target="tpu_custom_call" | custom-call | tf_op jit(solution)/shard_map/middle/pallas_call | solution.py:464
  64.2 6.9 %state1.1 = (f32[2,4096,128]{2,1,0:T(8,128)}, bf16[128,64]{1,0:T(8,128)(2,1)}) custom-call(bf16[128,384]{1,0:T(8,128)(2,1)} %get-tuple-element.19.proj, f32[1,64]{1,0:T(1,128)} %get-tuple-element.31.base, f32[1,64]{1,0:T(1,128)} %get-tuple-element.26.ggain, f32[2,4096,128]{2,1,0:T(8,128)} %bitcast.9, ...), custom_call_target="tpu_custom_call", output_to_operand_aliasing={{0}: (4, {})} | custom-call | tf_op jit(solution)/shard_map/state1/pallas_call | solution.py:441
  71.1 28.4 %last.1 = bf16[256,2048]{1,0:T(8,128)(2,1)} custom-call(bf16[128,64]{1,0:T(8,128)(2,1)} %get-tuple-element.21.mixed, bf16[16,2,64,256]{3,2,1,0:T(8,128)(2,1)} %get-tuple-element.15.outw, bf16[128,256]{1,0:T(8,128)(2,1)} %get-tuple-element.22.near), custom_call_target="tpu_custom_call" | custom-call | tf_op jit(solution)/shard_map/last/pallas_call | solution.py:474
  99.5 2.3 %copy.18 = bf16[256,2048]{1,0:T(8,128)(2,1)} copy(bf16[256,2048]{1,0:T(8,128)(2,1)} %last.1) | data formatting | bytes 2097152

commit v2 on v1

--- a/solution.py
+++ b/solution.py
@@ -136,7 +136,7 @@
         return [(p, self.d) for p in near + [self.at(self.x, self.y, dz) for dz in range(1, self.nz)]]
 
 
-def gather(lanes, buf, send, recv):
+def gather(lanes, buf, send, recv, beside=None, arrived=None):
     x, y, nz, d = lanes.x, lanes.y, lanes.nz, lanes.d
     xp, yp = lanes.at(1 - x, y, 0), lanes.at(x, 1 - y, 0)
     started = []
@@ -150,6 +150,8 @@
 
     def got(half, block):
         remote(buf.at[half, block], buf.at[half, block], send.at[half, 0], recv.at[half, block], xp, d).wait_recv()
+        if arrived is not None:
+            arrived(half, block)
 
     zs = list(range(1, nz))
     own = lanes.t
@@ -160,6 +162,8 @@
     put(1, own, xp)
     put(1, own, yp)
     put(0, own, xp)
+    if beside is not None:
+        beside()
     got(0, yp)
     for dz in zs:
         put(0, yp, lanes.at(x, y, dz))
@@ -190,7 +194,7 @@
 
 def first_kernel(
     tp, tok, gain, wr, wk, wv, wd, wa, wg, wo, proj, near, w1, gain1, outw,
-    tokv, w0, part, inbox, load, send, recv, a2a_send, a2a_recv,
+    tokv, w0, part, inbox, load, send, recv, a2a_send, a2a_recv, on_send, on_recv,
 ):
     lanes = Lanes(tp)
     t, d = lanes.t, lanes.d
@@ -258,15 +262,17 @@
     here = (t // per == d).astype(jnp.float32)
     near[...] = (own.astype(jnp.float32) * here + near[...].astype(jnp.float32) * (1.0 - here)).astype(jnp.bfloat16)
 
-    forward = remote(outw, outw, send.at[9], recv.at[9], t, 1 - d)
+    def forward(source):
+        return remote(outw.at[source], outw.at[source], on_send.at[source], on_recv.at[source], t, 1 - d)
 
     @pl.when(t // per == d)
     def _():
+        pltpu.make_async_copy(outw.at[t], outw.at[t], a2a_send.at[slot]).wait()
+        forward(t).start()
         for k in range(1, tp):
             source = lax.rem(t + k, tp)
             remote(outw.at[source], outw.at[source], a2a_send.at[0], a2a_recv.at[source], t, 1 - d).wait_recv()
-        pltpu.make_async_copy(outw.at[t], outw.at[t], a2a_send.at[slot]).wait()
-        forward.start()
+            forward(source).start()
 
     for c in range(per):
         @pl.when(d * per + c != t)
@@ -275,11 +281,13 @@
 
     @pl.when(t // per == d)
     def _():
-        forward.wait_send()
+        for k in range(tp):
+            forward(k).wait_send()
 
     @pl.when(t // per != d)
     def _():
-        forward.wait_recv()
+        for k in range(tp):
+            forward(k).wait_recv()
 
     for op in pair[1:]:
         op.wait_recv()
@@ -348,12 +356,18 @@
     for k in range(2):
         mg[k, lanes.t] = heads[k * half // 2 : (k + 1) * half // 2]
     greet(lanes.peers() + [(lanes.t, 1 - lanes.d)])
-    we[...] = jnp.zeros_like(we)
-    for k in range(tp):
-        block = outw[k, layer]
-        we[k * 2 * HEAD : k * 2 * HEAD + HEAD, 0:cols] = block
-        we[k * 2 * HEAD + HEAD : (k + 1) * 2 * HEAD, cols : 2 * cols] = block
-    gather(lanes, mg, send, recv)
+
+    def place():
+        zero = jnp.zeros((HEAD, cols), we.dtype)
+        for k in range(tp):
+            block = outw[k, layer]
+            top, bottom = pl.ds(k * 2 * HEAD, HEAD), pl.ds(k * 2 * HEAD + HEAD, HEAD)
+            we[top, 0:cols] = block
+            we[top, cols : 2 * cols] = zero
+            we[bottom, 0:cols] = zero
+            we[bottom, cols : 2 * cols] = block
+
+    gather(lanes, mg, send, recv, beside=place)
     packed = jnp.concatenate(
         [jnp.concatenate([mg[k, j] for j in range(tp)], axis=1) for k in range(2)], axis=0
     )
@@ -362,8 +376,10 @@
     return (near[...].astype(jnp.float32) + out).astype(jnp.bfloat16)
 
 
-def middle_kernel(tp, mixed, outw, near, w1, gain1, proj, after, mg, we, xg, send, recv, xsend, xrecv):
+def middle_kernel(tp, mixed, outw, near, w1, gain1, proj, after, mg, we, xg, send, recv, xsend, xrecv, w1v, wsem):
     lanes = Lanes(tp)
+    load = pltpu.make_async_copy(w1, w1v, wsem)
+    load.start()
     current = project_out(lanes, tp, 0, mixed, outw, near, mg, we, send, recv)
     after[...] = current
     lane = current.shape[1] // 2
@@ -371,12 +387,13 @@
         xg[k, lanes.t] = current[:, k * lane : (k + 1) * lane]
     gather(lanes, xg, xsend, xrecv)
     per = tp // 2
+    load.wait()
     squares, part = 0.0, 0.0
     for e in range(2):
         floats = jnp.concatenate([xg[k, e * per + j] for j in range(per) for k in range(2)], axis=1).astype(jnp.float32)
         squares = squares + jnp.sum(floats * floats, axis=1, keepdims=True)
         normed = (floats * gain1[e, 1:2, :]).astype(jnp.bfloat16)
-        part = part + lax.dot_general(normed, w1[e], NT, preferred_element_type=jnp.float32)
+        part = part + lax.dot_general(normed, w1v[e], NT, preferred_element_type=jnp.float32)
     inv = lax.rsqrt(squares / (w1.shape[0] * w1.shape[2]) + norm_floor)
     proj[...] = (inv * part).astype(jnp.bfloat16)
 
@@ -388,18 +405,33 @@
     d, per = lanes.d, tp // 2
     for k in range(2):
         xg[k, lanes.t] = current[:, k * lane : (k + 1) * lane]
-    gather(lanes, xg, xsend, xrecv)
-    swap = remote(xg.at[:, pl.ds((1 - d) * per, per)], xo, osend, orecv, lanes.t, 1 - d)
-    swap.start()
+
+    def hand(half, block):
+        place = lax.rem(block, per)
+        return remote(xg.at[half, block], xo.at[half, place], osend.at[half, place], orecv.at[half, place], lanes.t, 1 - d)
+
+    def arrived(half, block):
+        @pl.when(block // per == 1 - d)
+        def _():
+            hand(half, block).start()
+
+    arrived(0, lanes.t)
+    arrived(1, lanes.t)
+    gather(lanes, xg, xsend, xrecv, arrived=arrived)
     for j in range(per):
         for k in range(2):
             at = (2 * j + k) * lane
             final[pl.ds(pl.multiple_of(d * mine, mine), mine), at : at + lane] = xg[k, d * per + j]
-    swap.wait()
+    for j in range(per):
+        for k in range(2):
+            hand(k, (1 - d) * per + j).wait_recv()
     for j in range(per):
         for k in range(2):
             at = (2 * j + k) * lane
             final[pl.ds(pl.multiple_of((1 - d) * mine, mine), mine), at : at + lane] = xo[k, j]
+    for j in range(per):
+        for k in range(2):
+            hand(k, (1 - d) * per + j).wait_send()
 
 
 def fast(tp, tokens, norm_gain, projections, decay_base, group_gain, output_proj, state):
@@ -428,7 +460,8 @@
         out_specs=(vm,) * 5,
         scratch_shapes=[
             pltpu.VMEM((rows, feats), bf), pltpu.VMEM((width, feats), bf), pltpu.VMEM((rows, width + 128), f32),
-            pltpu.VMEM((mine, width + 128), f32), dma((13,)), dma((10,)), dma((10,)), dma((per,)), dma((tp,)),
+            pltpu.VMEM((mine, width + 128), f32), dma((13,)), dma((9,)), dma((9,)), dma((per,)), dma((tp,)),
+            dma((tp,)), dma((tp,)),
         ],
         compiler_params=params(0),
         name="first",
@@ -464,9 +497,9 @@
     proj, near = pl.pallas_call(
         functools.partial(middle_kernel, tp),
         out_shape=(shape((mine, width), bf), shape((mine, cols), bf)),
-        in_specs=[vm] * 5,
+        in_specs=[vm] * 3 + [anywhere, vm],
         out_specs=(vm,) * 2,
-        scratch_shapes=common + sems,
+        scratch_shapes=common + sems + [pltpu.VMEM(w1.shape, bf), dma],
         compiler_params=params(1),
         name="middle",
     )(mixed, outw, near, w1, gain1)
@@ -476,7 +509,7 @@
         out_shape=shape((rows, feats), bf),
         in_specs=[vm] * 3,
         out_specs=vm,
-        scratch_shapes=common + [pltpu.VMEM((2, per, mine, cols // 2), bf)] + sems + [dma, dma],
+        scratch_shapes=common + [pltpu.VMEM((2, per, mine, cols // 2), bf)] + sems + [dma((2, per)), dma((2, per))],
         compiler_params=params(2),
         name="last",
     )(mixed, outw, near)

time: 102 us -> 100 us (0.980)
  Pallas kernels: 97.5 us -> 95.7 us
where the time goes in v2:
time: 100 us
  Pallas kernels  95.7 us (96%)
  local copies, waits for them, and re-layouts  3.65 us (4%)
    pallas_call x1, Pallas kernels, fast(): pl.pallas_call(functools.partial(middle_kernel, tp), out_shape=(shape((mi...  33.9 us
    pallas_call x1, Pallas kernels, fast(): pl.pallas_call(functools.partial(last_kernel, tp), out_shape=shape((rows,...  27.9 us
    pallas_call x1, Pallas kernels, fast(): pl.pallas_call(functools.partial(first_kernel, tp), out_shape=(shape((min...  20.2 us
    pallas_call x2, Pallas kernels, recur(): pl.pallas_call(state_kernel, grid=(mine // seqs,), out_shape=(shape(flat....  13.7 us
    unnamed x1, local copies, waits for them, and re-layouts  2.3 us

profile of v2, /device:TPU:0, one launch (start us, length us, event | category | flops | bytes accessed | tf_op | source)
XLA Modules:
  0.0 100.0 jit_solution(4460688760534653673)
XLA Ops:
  0.6 1.4 %fusion = (f32[1,64]{1,0:T(1,128)}, f32[1,64]{1,0:T(1,128)}, f32[1,64]{1,0:T(1,128)}, f32[1,64]{1,0:T(1,128)}) fusion(f32[2,64]{1,0:T(2,128)} %param.21, f32[2,64]{1,0:T(2,128)} %param.20), kind=kLoop, calls=%fused_computation | loop fusion | bytes 2048 | tf_op jit(solution)/shard_map/slice | solution.py:491
  2.0 20.2 %first.1 = (bf16[128,384]{1,0:T(8,128)(2,1)}, bf16[128,256]{1,0:T(8,128)(2,1)}, bf16[2,384,2048]{2,1,0:T(8,128)(2,1)}, f32[2,2,2048]{2,1,0:T(2,128)}, bf16[16,2,64,256]{3,2,1,0:T(8,128)(2,1)}) custom-call(bf16[256,2048]{1,0:T(8,128)(2,1)} %tok.1, f32[2,2048]{1,0:T(2,128)} %gain.1, bf16[2,64,2048]{2,1,0:T(8,128)(2,1)} %bitcast.11, ...), custom_call_target="tpu_custom_call" | custom-call | tf_op jit(solution)/shard_map/first/pallas_call | solution.py:453
  22.2 6.9 %state0.1 = (f32[2,4096,128]{2,1,0:T(8,128)}, bf16[128,64]{1,0:T(8,128)(2,1)}) custom-call(bf16[128,384]{1,0:T(8,128)(2,1)} %get-tuple-element.13.proj, f32[1,64]{1,0:T(1,128)} %get-tuple-element.30.base, f32[1,64]{1,0:T(1,128)} %get-tuple-element.27.ggain, f32[2,4096,128]{2,1,0:T(8,128)} %bitcast.8), custom_call_target="tpu_custom_call" | custom-call | tf_op jit(solution)/shard_map/state0/pallas_call | solution.py:474
  29.1 33.9 %middle.1 = (bf16[128,384]{1,0:T(8,128)(2,1)}, bf16[128,256]{1,0:T(8,128)(2,1)}) custom-call(bf16[128,64]{1,0:T(8,128)(2,1)} %get-tuple-element.14.mixed, bf16[16,2,64,256]{3,2,1,0:T(8,128)(2,1)} %get-tuple-element.15.outw, bf16[128,256]{1,0:T(8,128)(2,1)} %get-tuple-element.16.near, bf16[2,384,2048]{2,1,0:T(8,128)(2,1)} %get-tuple-element.17.w1, ...), custom_call_target="tpu_custom_call" | custom-call | tf_op jit(solution)/shard_map/middle/pallas_call | solution.py:497
  62.9 6.9 %state1.1 = (f32[2,4096,128]{2,1,0:T(8,128)}, bf16[128,64]{1,0:T(8,128)(2,1)}) custom-call(bf16[128,384]{1,0:T(8,128)(2,1)} %get-tuple-element.19.proj, f32[1,64]{1,0:T(1,128)} %get-tuple-element.31.base, f32[1,64]{1,0:T(1,128)} %get-tuple-element.26.ggain, f32[2,4096,128]{2,1,0:T(8,128)} %bitcast.9, ...), custom_call_target="tpu_custom_call", output_to_operand_aliasing={{0}: (4, {})} | custom-call | tf_op jit(solution)/shard_map/state1/pallas_call | solution.py:474
  69.8 27.9 %last.1 = bf16[256,2048]{1,0:T(8,128)(2,1)} custom-call(bf16[128,64]{1,0:T(8,128)(2,1)} %get-tuple-element.21.mixed, bf16[16,2,64,256]{3,2,1,0:T(8,128)(2,1)} %get-tuple-element.15.outw, bf16[128,256]{1,0:T(8,128)(2,1)} %get-tuple-element.22.near), custom_call_target="tpu_custom_call" | custom-call | tf_op jit(solution)/shard_map/last/pallas_call | solution.py:507
  97.7 2.3 %copy.18 = bf16[256,2048]{1,0:T(8,128)(2,1)} copy(bf16[256,2048]{1,0:T(8,128)(2,1)} %last.1) | data formatting | bytes 2097152

commit v3 on v2

--- a/solution.py
+++ b/solution.py
@@ -213,16 +213,18 @@
 
     def spread(c):
         target = d * per + c
-        return remote(wo.at[:, :, pl.ds(c * cols, cols)], outw.at[t], a2a_send.at[c], a2a_recv.at[t], target, d)
-
-    for c in range(per):
+        return remote(wo.at[:, :, pl.ds(pl.multiple_of(c * cols, cols), cols)], outw.at[t], a2a_send.at[c], a2a_recv.at[t], target, d)
+
+    for k in range(per):
+        c = lax.rem(t + k, per)
+
         @pl.when(d * per + c != t)
         def _(c=c):
             spread(c).start()
 
         @pl.when(d * per + c == t)
         def _(c=c):
-            pltpu.make_async_copy(wo.at[:, :, pl.ds(c * cols, cols)], outw.at[t], a2a_send.at[c]).start()
+            pltpu.make_async_copy(wo.at[:, :, pl.ds(pl.multiple_of(c * cols, cols), cols)], outw.at[t], a2a_send.at[c]).start()
 
     loads[0].wait()
     slot = lax.rem(t, per)

time: 100 us -> 101 us (1.010)
    pallas_call x1, Pallas kernels: 33.9 us -> 28.5 us  [fast(): pl.pallas_call(functools.partial(middle_kernel, tp), out_shape=(shape((mi...]
    pallas_call x1, Pallas kernels: 20.2 us -> 25.5 us  [fast(): pl.pallas_call(functools.partial(first_kernel, tp), out_shape=(shape((min...]
where the time goes in v3:
time: 101 us; the launch traced here: 100 us
  Pallas kernels  96.1 us (95%)
  local copies, waits for them, and re-layouts  3.65 us (4%)
    pallas_call x1, Pallas kernels, fast(): pl.pallas_call(functools.partial(middle_kernel, tp), out_shape=(shape((mi...  28.5 us
    pallas_call x1, Pallas kernels, fast(): pl.pallas_call(functools.partial(last_kernel, tp), out_shape=shape((rows,...  28.3 us
    pallas_call x1, Pallas kernels, fast(): pl.pallas_call(functools.partial(first_kernel, tp), out_shape=(shape((min...  25.5 us
    pallas_call x2, Pallas kernels, recur(): pl.pallas_call(state_kernel, grid=(mine // seqs,), out_shape=(shape(flat....  13.7 us
    unnamed x1, local copies, waits for them, and re-layouts  2.3 us

profile of v3, /device:TPU:0, one launch (start us, length us, event | category | flops | bytes accessed | tf_op | source)
XLA Modules:
  0.0 100.4 jit_solution(400443417289126162)
XLA Ops:
  0.6 1.4 %fusion = (f32[1,64]{1,0:T(1,128)}, f32[1,64]{1,0:T(1,128)}, f32[1,64]{1,0:T(1,128)}, f32[1,64]{1,0:T(1,128)}) fusion(f32[2,64]{1,0:T(2,128)} %param.21, f32[2,64]{1,0:T(2,128)} %param.20), kind=kLoop, calls=%fused_computation | loop fusion | bytes 2048 | tf_op jit(solution)/shard_map/slice | solution.py:493
  2.0 25.5 %first.1 = (bf16[128,384]{1,0:T(8,128)(2,1)}, bf16[128,256]{1,0:T(8,128)(2,1)}, bf16[2,384,2048]{2,1,0:T(8,128)(2,1)}, f32[2,2,2048]{2,1,0:T(2,128)}, bf16[16,2,64,256]{3,2,1,0:T(8,128)(2,1)}) custom-call(bf16[256,2048]{1,0:T(8,128)(2,1)} %tok.1, f32[2,2048]{1,0:T(2,128)} %gain.1, bf16[2,64,2048]{2,1,0:T(8,128)(2,1)} %bitcast.11, ...), custom_call_target="tpu_custom_call" | custom-call | tf_op jit(solution)/shard_map/first/pallas_call | solution.py:455
  27.5 6.9 %state0.1 = (f32[2,4096,128]{2,1,0:T(8,128)}, bf16[128,64]{1,0:T(8,128)(2,1)}) custom-call(bf16[128,384]{1,0:T(8,128)(2,1)} %get-tuple-element.13.proj, f32[1,64]{1,0:T(1,128)} %get-tuple-element.30.base, f32[1,64]{1,0:T(1,128)} %get-tuple-element.27.ggain, f32[2,4096,128]{2,1,0:T(8,128)} %bitcast.8), custom_call_target="tpu_custom_call" | custom-call | tf_op jit(solution)/shard_map/state0/pallas_call | solution.py:476
  34.4 28.5 %middle.1 = (bf16[128,384]{1,0:T(8,128)(2,1)}, bf16[128,256]{1,0:T(8,128)(2,1)}) custom-call(bf16[128,64]{1,0:T(8,128)(2,1)} %get-tuple-element.14.mixed, bf16[16,2,64,256]{3,2,1,0:T(8,128)(2,1)} %get-tuple-element.15.outw, bf16[128,256]{1,0:T(8,128)(2,1)} %get-tuple-element.16.near, bf16[2,384,2048]{2,1,0:T(8,128)(2,1)} %get-tuple-element.17.w1, ...), custom_call_target="tpu_custom_call" | custom-call | tf_op jit(solution)/shard_map/middle/pallas_call | solution.py:499
  62.9 6.9 %state1.1 = (f32[2,4096,128]{2,1,0:T(8,128)}, bf16[128,64]{1,0:T(8,128)(2,1)}) custom-call(bf16[128,384]{1,0:T(8,128)(2,1)} %get-tuple-element.19.proj, f32[1,64]{1,0:T(1,128)} %get-tuple-element.31.base, f32[1,64]{1,0:T(1,128)} %get-tuple-element.26.ggain, f32[2,4096,128]{2,1,0:T(8,128)} %bitcast.9, ...), custom_call_target="tpu_custom_call", output_to_operand_aliasing={{0}: (4, {})} | custom-call | tf_op jit(solution)/shard_map/state1/pallas_call | solution.py:476
  69.8 28.3 %last.1 = bf16[256,2048]{1,0:T(8,128)(2,1)} custom-call(bf16[128,64]{1,0:T(8,128)(2,1)} %get-tuple-element.21.mixed, bf16[16,2,64,256]{3,2,1,0:T(8,128)(2,1)} %get-tuple-element.15.outw, bf16[128,256]{1,0:T(8,128)(2,1)} %get-tuple-element.22.near), custom_call_target="tpu_custom_call" | custom-call | tf_op jit(solution)/shard_map/last/pallas_call | solution.py:509
  98.1 2.3 %copy.18 = bf16[256,2048]{1,0:T(8,128)(2,1)} copy(bf16[256,2048]{1,0:T(8,128)(2,1)} %last.1) | data formatting | bytes 2097152
